TPU v7x, 512 devices: a whole 4x4x16 slice. The times are simulated.
512 devices in a mesh: sp: 32 (over z, core), tp: 16 (over y, x).
Axes of the slice: x: 4, y: 4, z: 16, core: 2. Of those that a mesh axis runs over, the one named last changes fastest.
Arguments:
- resid: bfloat16 [6144, 2048], P('sp', 'tp'), may hold values from -12 to 12
- conv_value: bfloat16 [6144, 2048], P('sp', 'tp'), may hold values from -80 to 80
- conv_gate: bfloat16 [6144, 2048], P('sp', 'tp'), may hold values from -6 to 6
- depth_kernel: float32 [31, 2048], P(None, 'tp'), may hold values from -1 to 1
- chan_gain: float32 [2048], P('tp'), may hold values from 0.1 to 1.9
- point_weight: bfloat16 [2048, 2048], P('tp'), may hold values from -0.125 to 0.125
- mix_gain: float32 [2048], replicated, may hold values from 0.1 to 1.9
- out_weight: bfloat16 [2048, 2048], P(None, 'tp'), may hold values from -0.125 to 0.125
- norm_gain: float32 [2048], P('tp'), may hold values from 0.1 to 1.9
- route_ids: int32 [6144, 4], P('sp'), may hold values from 0 to 31, all different within a row; in each aligned block of 192 rows (0 to 191, 192 to 383, ...) at most 32 rows name the same one
- route_weights: float32 [6144, 4], P('sp'), may hold values from 0.05 to 0.5
- gate_experts: bfloat16 [32, 2048, 4096], P('sp', None, 'tp'), may hold values from -0.3125 to 0.3125
- up_experts: bfloat16 [32, 2048, 4096], P('sp', None, 'tp'), may hold values from -0.3125 to 0.3125
- down_experts: bfloat16 [32, 4096, 2048], P('sp', 'tp'), may hold values from -0.09375 to 0.09375
Outputs:
- result: bfloat16 [6144, 2048], P('sp', 'tp')
Inputs may be any that keep to these rules, and one draw needn't show every extreme that they name: `route_ids`: each row names 4 different experts; among the 192 rows of one index of sp no expert is named by more than 32 rows, and in some such block an expert is named by exactly 32.
All inputs are finite; a program needn't handle non-finite values.
Results may differ from a plain program's by a relative error of at most 0.024.
Values may be sent and summed in bfloat16 or wider, within the bound.
A program may use at most 64 MiB of HBM per device.

v0:
```python
import jax
import jax.numpy as jnp
from jax import lax
from jax.sharding import Mesh
from jax.sharding import PartitionSpec as P

E = 32
TOPK = 4
CAP = 32
TP = ("tp_0", "tp_1")
epsilon = 1e-05
clamp_limit = 7.0
swish_slope = 1.702


def from_behind(block, axis, distance):
    devices = range(lax.axis_size(axis))
    route = [(i - distance, i) for i in devices if i - distance in devices]
    return lax.ppermute(block, axis, route)


def over_axes(value, axes):
    for axis in axes:
        value = lax.psum(value, axis)
    return value


def split_up(value, dim, count):
    dims = value.shape
    pieces = value.reshape(*dims[:dim], count, dims[dim] // count, *dims[dim + 1 :])
    return jnp.moveaxis(pieces, dim, 0)


def summed_on_arrival(value, axis, dim):
    pieces = split_up(value, dim, lax.axis_size(axis))
    arrived = lax.all_to_all(pieces, axis, split_axis=0, concat_axis=0, tiled=True)
    return arrived.astype(jnp.float32).sum(axis=0)


def from_everyone(value, axis):
    copies = jnp.broadcast_to(value, (lax.axis_size(axis), *value.shape))
    return lax.all_to_all(copies, axis, split_axis=0, concat_axis=0, tiled=True)


def laid_out(pieces, dim):
    dims = list(pieces.shape[1:])
    dims[dim] *= pieces.shape[0]
    return jnp.moveaxis(pieces, 0, dim).reshape(dims)


def gathered_copies(value, axis, dim):
    pieces = from_everyone(value, axis)
    return laid_out(pieces, dim)


def shards(
    resid,
    conv_value,
    conv_gate,
    depth_kernel,
    chan_gain,
    point_weight,
    mix_gain,
    out_weight,
    norm_gain,
    route_ids,
    route_weights,
    gate_experts,
    up_experts,
    down_experts,
):
    tok_rows, chan_local = conv_value.shape
    feat_local = resid.shape[1]
    lookback = depth_kernel.shape[0] - 1
    gated = (conv_value.astype(jnp.float32) * jax.nn.sigmoid(conv_gate.astype(jnp.float32))).astype(
        jnp.bfloat16
    )
    earlier = from_behind(gated[tok_rows - lookback :], "sp", 1)
    padded = jnp.concatenate([earlier, gated], axis=0)
    conv = jnp.zeros((tok_rows, chan_local), jnp.float32)
    for tap in range(lookback + 1):
        conv = conv + padded[tap : tap + tok_rows].astype(jnp.float32) * depth_kernel[tap]
    chan_total = chan_local * lax.axis_size(TP)
    row_sums, row_squares = (
        over_axes(jnp.sum(conv, axis=1), TP),
        over_axes(jnp.sum(conv * conv, axis=1), TP),
    )
    row_mean = row_sums / chan_total
    row_var = row_squares / chan_total - row_mean * row_mean
    act = jax.nn.silu(
        (conv - row_mean[:, None]) * lax.rsqrt(row_var[:, None] + epsilon) * chan_gain
    ).astype(jnp.bfloat16)
    point = summed_on_arrival(
        jnp.dot(act, point_weight, preferred_element_type=jnp.float32).astype(jnp.bfloat16), TP, 0
    )
    mixed = (
        point * lax.rsqrt(jnp.mean(point * point, axis=1, keepdims=True) + epsilon) * mix_gain
    ).astype(jnp.bfloat16)
    branch = jnp.dot(gathered_copies(mixed, TP, 0), out_weight, preferred_element_type=jnp.float32)
    middle = (resid.astype(jnp.float32) + branch).astype(jnp.bfloat16)
    middle32 = middle.astype(jnp.float32)
    feat_total = feat_local * lax.axis_size(TP)
    squares = over_axes(jnp.sum(middle32 * middle32, axis=1), TP)
    normed = (middle32 * lax.rsqrt(squares[:, None] / feat_total + epsilon) * norm_gain).astype(
        jnp.bfloat16
    )
    flat_ids = route_ids.reshape(-1)
    expert_table = (flat_ids[:, None] == jnp.arange(E, dtype=jnp.int32)[None, :]).astype(jnp.int32)
    earlier_count = jnp.cumsum(expert_table, axis=0) - expert_table
    position = jnp.sum(earlier_count * expert_table, axis=1)
    slot_of = flat_ids * CAP + position
    slot_grid = slot_of.reshape(tok_rows, TOPK)
    picker = jnp.any(
        slot_grid[None, :, :] == jnp.arange(E * CAP, dtype=jnp.int32)[:, None, None], axis=2
    ).astype(jnp.bfloat16)
    outgoing = (
        jnp.dot(picker, normed, preferred_element_type=jnp.float32)
        .astype(jnp.bfloat16)
        .reshape(E, CAP, feat_local)
    )
    received = lax.all_gather(
        lax.all_to_all(outgoing, "sp", split_axis=0, concat_axis=0, tiled=True),
        TP,
        axis=2,
        tiled=True,
    )
    local_experts = gate_experts.shape[0]
    sources = received.shape[0] // local_experts
    count = received.shape[1]
    rows = received.reshape(sources, local_experts, count, received.shape[2])
    gate_pre = jnp.minimum(
        jnp.einsum("sjcd,jdf->sjcf", rows, gate_experts, preferred_element_type=jnp.float32),
        clamp_limit,
    )
    up_pre = jnp.clip(
        jnp.einsum("sjcd,jdf->sjcf", rows, up_experts, preferred_element_type=jnp.float32),
        -clamp_limit,
        clamp_limit,
    )
    hidden = (gate_pre * jax.nn.sigmoid(swish_slope * gate_pre) * (up_pre + 1.0)).astype(
        jnp.bfloat16
    )
    partial_value = jnp.einsum(
        "sjcf,jfd->sjcd", hidden, down_experts, preferred_element_type=jnp.float32
    )
    summed = summed_on_arrival(partial_value.astype(jnp.bfloat16), TP, 3).astype(jnp.bfloat16)
    returned = lax.all_to_all(
        summed.reshape(sources * local_experts, count, summed.shape[3]),
        "sp",
        split_axis=0,
        concat_axis=0,
        tiled=True,
    )
    flat_back = returned.reshape(E * CAP, feat_local)
    picked = flat_back[slot_of].astype(jnp.float32).reshape(tok_rows, TOPK, feat_local)
    routed_sum = jnp.sum(picked * route_weights[:, :, None], axis=1)
    return (middle32 + routed_sum).astype(jnp.bfloat16)


def solution(mesh):
    split = Mesh(mesh.devices.reshape(mesh.shape["sp"], 4, 4), ("sp", "tp_0", "tp_1"))
    return jax.shard_map(
        shards,
        mesh=split,
        in_specs=(
            P("sp", TP),
            P("sp", TP),
            P("sp", TP),
            P(None, TP),
            P(TP),
            P(TP, None),
            P(),
            P(None, TP),
            P(TP),
            P("sp", None),
            P("sp", None),
            P("sp", None, TP),
            P("sp", None, TP),
            P("sp", TP, None),
        ),
        out_specs=P("sp", TP),
        check_vma=False,
    )
```

profile of v0, /device:TPU:1, one launch (start us, length us, event | category | flops | bytes accessed | tf_op | source)
XLA Modules:
  0.0 313.9 jit_solution(2929535783332254951)
XLA Ops:
  6.5 0.0 copy-start
  6.5 0.0 copy-start.6
  6.5 0.0 copy-start.5
  6.5 0.9 multiply_convert_fusion.3
  7.5 4.9 %collective-permute-start = (bf16[30,128]{1,0:T(8,128)(2,1)S(1)}, bf16[30,128]{1,0:T(8,128)(2,1)S(1)}, u32[]{:S(2)}, u32[]{:S(2)}) collective-permute-start(bf16[30,128]{1,0:T(8,128)(2,1)S(1)} %slice.258), channel_id=1, source_target_pairs={{0,16},{16,32},{32,48},{48,64},{64,80},{80,96},{96,112},{112,128},... | collective-permute-start | bytes 23048 | tf_op jit(solution)/shard_map/ppermute | solution.py:19
  12.4 1.0 slice_bitcast_fusion.30
  13.4 1.0 slice_bitcast_fusion.29
  14.4 1.9 collective-permute-done
  16.3 0.5 fusion.66
  16.8 7.1 %all-reduce.1 = (f32[192]{0:T(256)S(1)}, f32[192]{0:T(256)S(1)}) all-reduce(f32[192]{0:T(256)S(1)} %get-tuple-element.6, f32[192]{0:T(256)S(1)} %get-tuple-element.5), channel_id=1, replica_groups=mesh['sp'=32,'tp_0'=4,'tp_1'=4] {'tp_0'}, use_global_device_ids=true, to_apply=%region_4.0 | all-reduce | flops 384 | bytes 3072 | tf_op jit(solution)/shard_map/psum | solution.py:24
  23.9 8.2 %all-reduce = (f32[192]{0:T(256)S(1)}, f32[192]{0:T(256)S(1)}) all-reduce(f32[192]{0:T(256)S(1)} %get-tuple-element.9, f32[192]{0:T(256)S(1)} %get-tuple-element.10), channel_id=1, replica_groups=mesh['sp'=32,'tp_0'=4,'tp_1'=4] {'tp_1'}, use_global_device_ids=true, to_apply=%region_5.0 | all-reduce | flops 384 | bytes 3072 | tf_op jit(solution)/shard_map/psum | solution.py:24
  32.1 1.5 convolution_convert_fusion
  33.6 1.2 reshape.122
  34.8 3.7 %all-to-all-start = ((bf16[16,12,2048]{2,1,0:T(8,128)(2,1)}), bf16[16,12,2048]{2,1,0:T(8,128)(2,1)S(1)}, u32[]{:S(2)}, u32[]{:S(2)}) async-start(bf16[16,12,2048]{2,1,0:T(8,128)(2,1)} %reshape.122), calls=%async_computation | async-start | bytes 2097152 | tf_op jit(solution)/shard_map/all_to_all | solution.py:36
  38.5 0.0 copy-done.6
  38.5 0.0 copy-start.1
  38.5 0.0 copy-start.2
  38.5 0.1 copy.28
  38.6 0.1 eq.42
  38.7 0.1 eq.38
  38.8 14.4 %all-to-all-done = bf16[16,12,2048]{2,1,0:T(8,128)(2,1)S(1)} async-done(((bf16[16,12,2048]{2,1,0:T(8,128)(2,1)}), bf16[16,12,2048]{2,1,0:T(8,128)(2,1)S(1)}, u32[]{:S(2)}, u32[]{:S(2)}) %all-to-all-start) | async-done | bytes 786464 | tf_op jit(solution)/shard_map/all_to_all | solution.py:36
  53.2 0.2 convert_reduce_fusion
  53.4 0.1 multiply_reduce_fusion
  53.5 0.0 copy-done.5
  53.5 0.1 multiply_convert_fusion
  53.6 1.1 broadcast_in_dim.2
  54.7 3.7 %all-to-all-start.1 = ((bf16[16,12,2048]{2,1,0:T(8,128)(2,1)}), bf16[16,12,2048]{2,1,0:T(8,128)(2,1)S(1)}, u32[]{:S(2)}, u32[]{:S(2)}) async-start(bf16[16,12,2048]{2,1,0:T(8,128)(2,1)} %broadcast_in_dim.2), calls=%async_computation.1 | async-start | bytes 2097152 | tf_op jit(solution)/shard_map/all_to_all | solution.py:42
  58.5 0.0 all-gather.2.cloned.1.call-start
  58.5 1.7 reduce-window.6
  60.3 0.3 slice_reduce_fusion
  60.6 0.1 fusion.22
  60.7 0.0 copy-start.3
  60.7 0.6 copy-done.3
  61.3 0.1 reduce_sum.84
  61.4 0.1 copy.32
  61.5 1.2 fusion
  62.7 9.5 %all-to-all-done.1 = bf16[16,12,2048]{2,1,0:T(8,128)(2,1)S(1)} async-done(((bf16[16,12,2048]{2,1,0:T(8,128)(2,1)}), bf16[16,12,2048]{2,1,0:T(8,128)(2,1)S(1)}, u32[]{:S(2)}, u32[]{:S(2)}) %all-to-all-start.1) | async-done | bytes 786464 | tf_op jit(solution)/shard_map/all_to_all | solution.py:42
  72.2 0.2 reshape.123
  72.4 0.0 copy-done.1
  72.4 0.0 copy-done.2
  72.4 0.5 multiply_reduce_fusion.1
  72.8 7.3 %psum.46 = f32[192]{0:T(256)S(1)} all-reduce(f32[192]{0:T(256)S(1)} %get-tuple-element.47), channel_id=1, replica_groups=mesh['sp'=32,'tp_0'=4,'tp_1'=4] {'tp_0'}, use_global_device_ids=true, to_apply=%region_13.14 | all-reduce | flops 192 | bytes 1536 | tf_op jit(solution)/shard_map/psum | solution.py:24
  80.1 6.6 %psum.47 = f32[192]{0:T(256)S(1)} all-reduce(f32[192]{0:T(256)S(1)} %psum.46), channel_id=1, replica_groups=mesh['sp'=32,'tp_0'=4,'tp_1'=4] {'tp_1'}, use_global_device_ids=true, to_apply=%region_14.15 | all-reduce | flops 192 | bytes 1536 | tf_op jit(solution)/shard_map/psum | solution.py:24
  86.7 1.4 convolution_convert_fusion.1
  88.2 44.7 %all_to_all.25 = bf16[32,32,128]{2,1,0:T(8,128)(2,1)} all-to-all(bf16[32,32,128]{2,1,0:T(8,128)(2,1)S(1)} %bitcast.146), channel_id=1, replica_groups=mesh['sp'=32,'tp_0'=4,'tp_1'=4] {'sp'}, dimensions={0} | all-to-all | bytes 524288 | tf_op jit(solution)/shard_map/all_to_all | solution.py:122
  132.9 0.0 all-gather.2.cloned.1.call-update
  132.9 0.0 copy-start.8
  132.9 58.5 %all-gather.2.cloned.1.call-done = bf16[32,32,2048]{2,1,0:T(8,128)(2,1)} async-done(((bf16[32,32,128]{2,1,0:T(8,128)(2,1)}), bf16[32,32,2048]{2,1,0:T(8,128)(2,1)}) %all-gather.2.cloned.1.call-update) | async-done | bytes 4194320 | tf_op jit(solution)/shard_map/all_gather | solution.py:121
  191.4 4.8 %fusion.1 = f32[32,1,32,256]{3,2,0,1:T(8,128)} fusion(bf16[32,32,2048]{2,1,0:T(8,128)(2,1)} %all-gather.2.cloned.1.call-done, bf16[1,2048,256]{2,1,0:T(8,128)(2,1)} %param.25), kind=kOutput, calls=%fused_computation.8 | convolution fusion | flops 1074003968 | bytes 6291456 | tf_op jit(solution)/shard_map/sjcd,jdf->sjcf/dot_general | solution.py:132
  196.2 0.0 copy-done
  196.2 0.0 copy-done.8
  196.2 8.9 %convert_bitcast_fusion = bf16[1,32,4,16,8,128]{5,4,3,2,1,0:T(8,128)(2,1)} fusion(bf16[1,256,2048]{2,1,0:T(8,128)(2,1)S(1)} %copy-done, bf16[32,32,2048]{2,1,0:T(8,128)(2,1)} %all-gather.2.cloned.1.call-done, bf16[1,2048,256]{2,1,0:T(8,128)(2,1)S(1)} %copy-done.8, f32[32,1,32,256]{3,2,0,1:T(8,128)} %fusion.1), kind=kOutput, calls=%fused_computation.2 | convolution fusion | flops 2151940096 | bytes 11534336 | tf_op jit(solution)/shard_map/sjcf,jfd->sjcd/dot_general | solution.py:143
  205.1 3.3 %copy.39 = bf16[1,32,4,16,8,128]{5,4,2,1,0,3:T(8,128)(2,1)S(1)} copy(bf16[1,32,4,16,8,128]{5,4,3,2,1,0:T(8,128)(2,1)} %convert_bitcast_fusion) | data formatting | bytes 8388608 | tf_op jit(solution)/shard_map/reshape | solution.py:30
  208.4 54.5 %all_to_all.26 = bf16[16,32,1,32,128]{4,3,1,2,0:T(8,128)(2,1)} all-to-all(bf16[16,32,1,32,128]{4,3,1,2,0:T(8,128)(2,1)S(1)} %bitcast.143), channel_id=1, replica_groups=mesh['sp'=32,'tp_0'=4,'tp_1'=4] {'tp_0','tp_1'}, dimensions={0} | all-to-all | bytes 8388608 | tf_op jit(solution)/shard_map/all_to_all | solution.py:36
  262.8 3.5 %reduce_sum.86 = bf16[32,32,128]{2,1,0:T(8,128)(2,1)} reduce(bf16[16,32,1,32,128]{4,3,1,2,0:T(8,128)(2,1)} %all_to_all.26, bf16[]{:T(256)} %constant.38.clone.1), dimensions={0,2}, to_apply=%region_15.16 | reduce | flops 1966080 | bytes 4456450 | tf_op jit(solution)/shard_map/reduce_sum | solution.py:37
  266.4 15.5 %all-to-all-start.4 = ((bf16[32,32,128]{2,1,0:T(8,128)(2,1)}), bf16[32,32,128]{2,1,0:T(8,128)(2,1)S(1)}, u32[]{:S(2)}, u32[]{:S(2)}) async-start(bf16[32,32,128]{2,1,0:T(8,128)(2,1)} %reduce_sum.86), calls=%async_computation.4 | async-start | bytes 524288 | tf_op jit(solution)/shard_map/all_to_all | solution.py:147
  281.9 0.1 mul.536
  282.0 0.0 copy-done.7
  282.0 0.1 copy.34
  282.1 0.0 copy-done.4
  282.2 22.0 %all-to-all-done.4 = bf16[32,32,128]{2,1,0:T(8,128)(2,1)S(1)} async-done(((bf16[32,32,128]{2,1,0:T(8,128)(2,1)}), bf16[32,32,128]{2,1,0:T(8,128)(2,1)S(1)}, u32[]{:S(2)}, u32[]{:S(2)}) %all-to-all-start.4) | async-done | bytes 262176 | tf_op jit(solution)/shard_map/all_to_all | solution.py:147
  304.2 1.9 gather_fusion
  306.0 0.3 fusion.19
  306.4 0.6 add_convert_fusion
  (11 shorter events, 0.1 us)
Async XLA Ops:
  6.5 189.7 %copy-start = (bf16[1,256,2048]{2,1,0:T(8,128)(2,1)S(1)}, bf16[1,256,2048]{2,1,0:T(8,128)(2,1)}, u32[]{:S(2)}) copy-start(bf16[1,256,2048]{2,1,0:T(8,128)(2,1)} %param.27) | copy-start | bytes 3145732
  6.5 31.9 %copy-start.6 = (s32[192,4]{0,1:T(4,128)S(1)}, s32[192,4]{0,1:T(4,128)}, u32[]{:S(2)}) copy-start(s32[192,4]{0,1:T(4,128)} %param.23) | copy-start | bytes 9220
  6.5 47.0 %copy-start.5 = (f32[2048]{0:T(1024)S(1)}, f32[2048]{0:T(1024)}, u32[]{:S(2)}) copy-start(f32[2048]{0:T(1024)} %param.20) | copy-start | bytes 24580
  7.5 8.8 %collective-permute-start = (bf16[30,128]{1,0:T(8,128)(2,1)S(1)}, bf16[30,128]{1,0:T(8,128)(2,1)S(1)}, u32[]{:S(2)}, u32[]{:S(2)}) collective-permute-start(bf16[30,128]{1,0:T(8,128)(2,1)S(1)} %slice.258), channel_id=1, source_target_pairs={{0,16},{16,32},{32,48},{48,64},{64,80},{80,96},{96,112},{112,128},... | collective-permute-start | bytes 23048 | tf_op jit(solution)/shard_map/ppermute | solution.py:19
  34.8 18.4 %all-to-all-start = ((bf16[16,12,2048]{2,1,0:T(8,128)(2,1)}), bf16[16,12,2048]{2,1,0:T(8,128)(2,1)S(1)}, u32[]{:S(2)}, u32[]{:S(2)}) async-start(bf16[16,12,2048]{2,1,0:T(8,128)(2,1)} %reshape.122), calls=%async_computation | async-start | bytes 2097152 | tf_op jit(solution)/shard_map/all_to_all | solution.py:36
  38.5 33.9 %copy-start.1 = (bf16[2048,128]{1,0:T(8,128)(2,1)S(1)}, bf16[2048,128]{1,0:T(8,128)(2,1)}, u32[]{:S(2)}) copy-start(bf16[2048,128]{1,0:T(8,128)(2,1)} %param.21) | copy-start | bytes 1572868
  38.5 33.9 %copy-start.2 = (bf16[192,128]{1,0:T(8,128)(2,1)S(1)}, bf16[192,128]{1,0:T(8,128)(2,1)}, u32[]{:S(2)}) copy-start(bf16[192,128]{1,0:T(8,128)(2,1)} %param.14) | copy-start | bytes 147460
  54.7 17.4 %all-to-all-start.1 = ((bf16[16,12,2048]{2,1,0:T(8,128)(2,1)}), bf16[16,12,2048]{2,1,0:T(8,128)(2,1)S(1)}, u32[]{:S(2)}, u32[]{:S(2)}) async-start(bf16[16,12,2048]{2,1,0:T(8,128)(2,1)} %broadcast_in_dim.2), calls=%async_computation.1 | async-start | bytes 2097152 | tf_op jit(solution)/shard_map/all_to_all | solution.py:42
  58.5 133.0 %all-gather.2.cloned.1.call-start = ((), (), s32[]{:S(2)}) async-start(), calls=%async_computation.5 | async-start | bytes 4456448 | tf_op jit(solution)/shard_map/all_gather | solution.py:121
  60.7 0.6 copy-start.3
  132.9 63.4 %copy-start.8 = (bf16[1,2048,256]{2,1,0:T(8,128)(2,1)S(1)}, bf16[1,2048,256]{2,1,0:T(8,128)(2,1)}, u32[]{:S(2)}) copy-start(bf16[1,2048,256]{2,1,0:T(8,128)(2,1)} %param.26) | copy-start | bytes 3145732
  262.8 19.2 %copy-start.7 = (f32[192,4]{0,1:T(4,128)S(1)}, f32[192,4]{0,1:T(4,128)}, u32[]{:S(2)}) copy-start(f32[192,4]{0,1:T(4,128)} %param.24) | copy-start | bytes 9220
  262.8 19.3 %copy-start.4 = (s32[768]{0:T(1024)S(1)}, s32[768]{0:T(1024)}, u32[]{:S(2)}) copy-start(s32[768]{0:T(1024)} %copy-done.3) | copy-start | bytes 9220
  266.4 37.8 %all-to-all-start.4 = ((bf16[32,32,128]{2,1,0:T(8,128)(2,1)}), bf16[32,32,128]{2,1,0:T(8,128)(2,1)S(1)}, u32[]{:S(2)}, u32[]{:S(2)}) async-start(bf16[32,32,128]{2,1,0:T(8,128)(2,1)} %reduce_sum.86), calls=%async_computation.4 | async-start | bytes 524288 | tf_op jit(solution)/shard_map/all_to_all | solution.py:147
Sparse Core Ops, SparseCore 0:
  133.0 58.3 all-gather.1
where the time goes:
time: 315 us; the launch traced here: 314 us
  blocking collectives  128 us (41%)
  waiting for transfers between devices  106 us (34%)
  starting transfers between devices  27.8 us (9%)
  matrix products  17 us (5%)
  between operations  13.7 us (4%)
  local copies, waits for them, and re-layouts  11.2 us (4%)
  other arithmetic  9.51 us (3%)
    all_gather x1, waiting for transfers between devices, shards(): lax.all_gather(lax.all_to_all(outgoing, 'sp', split_axis=0, concat_axis=0...  58.5 us
    all_to_all x1, blocking collectives, summed_on_arrival(): lax.all_to_all(pieces, axis, split_axis=0, concat_axis=0, tiled=True)  54.5 us
    all_to_all x1, blocking collectives, shards(): lax.all_to_all(outgoing, 'sp', split_axis=0, concat_axis=0, tiled=True)  44.7 us
    psum x4, blocking collectives, over_axes(): value = lax.psum(value, axis)  29.2 us
    all_to_all x1, waiting for transfers between devices, shards(): lax.all_to_all(summed.reshape(sources * local_experts, count, summed.shap...  22 us
    all_to_all x1, starting transfers between devices, shards(): lax.all_to_all(summed.reshape(sources * local_experts, count, summed.shap...  15.5 us
    all_to_all x1, waiting for transfers between devices, summed_on_arrival(): lax.all_to_all(pieces, axis, split_axis=0, concat_axis=0, tiled=True)  14.4 us
    all_to_all x1, waiting for transfers between devices, from_everyone(): return lax.all_to_all(copies, axis, split_axis=0, concat_axis=0, tiled=True)  9.49 us
  transfers between devices with their start and end apart: 5, of which 5 were waited for; matrix products, arithmetic and copies ran while one was open for 2% of the time, Pallas kernels for 0%

commit v1 on v0

--- a/solution.py
+++ b/solution.py
@@ -118,11 +118,17 @@
         .astype(jnp.bfloat16)
         .reshape(E, CAP, feat_local)
     )
-    received = lax.all_gather(
-        lax.all_to_all(outgoing, "sp", split_axis=0, concat_axis=0, tiled=True),
-        TP,
+    received = jnp.concatenate(
+        lax.all_to_all(
+            jnp.stack(
+                [lax.all_to_all(outgoing, "sp", split_axis=0, concat_axis=0, tiled=True)]
+                * lax.axis_size(TP)
+            ),
+            TP,
+            0,
+            0,
+        ),
         axis=2,
-        tiled=True,
     )
     local_experts = gate_experts.shape[0]
     sources = received.shape[0] // local_experts

time: 315 us -> 286 us (0.908)
  waiting for transfers between devices: 106 us -> 47.7 us
  blocking collectives: 128 us -> 180 us
  between operations: 13.7 us -> 0.27 us
  starting transfers between devices: 27.8 us -> 19.5 us
    all_gather x1 -> x0, waiting for transfers between devices: 58.5 us -> none  [shards(): lax.all_gather(lax.all_to_all(outgoing, 'sp', split_axis=0, concat_axis=0...]
    all_to_all x0 -> x1, blocking collectives: none -> 52.8 us  [shards(): lax.all_to_all(jnp.stack([lax.all_to_all(outgoing, 'sp', split_axis=0, co...]
    all_to_all x1, starting transfers between devices: 15.5 us -> 7.24 us  [shards(): lax.all_to_all(summed.reshape(sources * local_experts, count, summed.shap...]
  transfers between devices with their start and end apart: 5 -> 4, of which waited for: 5 -> 4; matrix products, arithmetic and copies ran while one was open for 2% -> 2% of each run, Pallas kernels for 0% -> 0%
where the time goes in v1:
time: 286 us; the launch traced here: 285 us
  blocking collectives  180 us (63%)
  waiting for transfers between devices  47.7 us (17%)
  starting transfers between devices  19.5 us (7%)
  matrix products  14.8 us (5%)
  local copies, waits for them, and re-layouts  13.9 us (5%)
  other arithmetic  9.51 us (3%)
    all_to_all x1, blocking collectives, summed_on_arrival(): lax.all_to_all(pieces, axis, split_axis=0, concat_axis=0, tiled=True)  53.1 us
    all_to_all x1, blocking collectives, shards(): lax.all_to_all(jnp.stack([lax.all_to_all(outgoing, 'sp', split_axis=0, co...  52.8 us
    all_to_all x1, blocking collectives, shards(): lax.all_to_all(outgoing, 'sp', split_axis=0, concat_axis=0, tiled=True)  44.6 us
    psum x4, blocking collectives, over_axes(): value = lax.psum(value, axis)  29.2 us
    all_to_all x1, waiting for transfers between devices, shards(): lax.all_to_all(summed.reshape(sources * local_experts, count, summed.shap...  22 us
    all_to_all x1, waiting for transfers between devices, summed_on_arrival(): lax.all_to_all(pieces, axis, split_axis=0, concat_axis=0, tiled=True)  14.4 us
    all_to_all x1, waiting for transfers between devices, from_everyone(): return lax.all_to_all(copies, axis, split_axis=0, concat_axis=0, tiled=True)  9.53 us
    dot_general x1, matrix products, shards(): jnp.einsum('sjcf,jfd->sjcd', hidden, down_experts, preferred_element_type...  9.12 us
  transfers between devices with their start and end apart: 4, of which 4 were waited for; matrix products, arithmetic and copies ran while one was open for 2% of the time, Pallas kernels for 0%

profile of v1, /device:TPU:1, one launch (start us, length us, event | category | flops | bytes accessed | tf_op | source)
XLA Modules:
  0.0 285.5 jit_solution(10509144264090167878)
XLA Ops:
  0.0 0.0 copy-start
  0.0 0.0 copy-start.7
  0.0 0.0 copy-start.6
  0.0 0.9 multiply_convert_fusion.3
  1.0 4.9 %collective-permute-start = (bf16[30,128]{1,0:T(8,128)(2,1)S(1)}, bf16[30,128]{1,0:T(8,128)(2,1)S(1)}, u32[]{:S(2)}, u32[]{:S(2)}) collective-permute-start(bf16[30,128]{1,0:T(8,128)(2,1)S(1)} %slice.258), channel_id=1, source_target_pairs={{0,16},{16,32},{32,48},{48,64},{64,80},{80,96},{96,112},{112,128},... | collective-permute-start | bytes 23048 | tf_op jit(solution)/shard_map/ppermute | solution.py:19
  5.9 1.0 slice_bitcast_fusion.30
  6.9 1.0 slice_bitcast_fusion.29
  7.9 1.9 collective-permute-done
  9.8 0.5 fusion.92
  10.3 7.1 %all-reduce.1 = (f32[192]{0:T(256)S(1)}, f32[192]{0:T(256)S(1)}) all-reduce(f32[192]{0:T(256)S(1)} %get-tuple-element.6, f32[192]{0:T(256)S(1)} %get-tuple-element.5), channel_id=1, replica_groups=mesh['sp'=32,'tp_0'=4,'tp_1'=4] {'tp_0'}, use_global_device_ids=true, to_apply=%region_4.0 | all-reduce | flops 384 | bytes 3072 | tf_op jit(solution)/shard_map/psum | solution.py:24
  17.4 8.2 %all-reduce = (f32[192]{0:T(256)S(1)}, f32[192]{0:T(256)S(1)}) all-reduce(f32[192]{0:T(256)S(1)} %get-tuple-element.9, f32[192]{0:T(256)S(1)} %get-tuple-element.10), channel_id=1, replica_groups=mesh['sp'=32,'tp_0'=4,'tp_1'=4] {'tp_1'}, use_global_device_ids=true, to_apply=%region_5.0 | all-reduce | flops 384 | bytes 3072 | tf_op jit(solution)/shard_map/psum | solution.py:24
  25.6 1.5 convolution_convert_fusion
  27.1 1.2 reshape.128
  28.3 3.7 %all-to-all-start = ((bf16[16,12,2048]{2,1,0:T(8,128)(2,1)}), bf16[16,12,2048]{2,1,0:T(8,128)(2,1)S(1)}, u32[]{:S(2)}, u32[]{:S(2)}) async-start(bf16[16,12,2048]{2,1,0:T(8,128)(2,1)} %reshape.128), calls=%async_computation | async-start | bytes 2097152 | tf_op jit(solution)/shard_map/all_to_all | solution.py:36
  31.9 0.0 copy-done.7
  31.9 0.0 copy-start.2
  32.0 0.0 copy-start.3
  32.0 0.1 copy.29
  32.1 0.1 eq.42
  32.2 0.1 eq.38
  32.3 14.4 %all-to-all-done = bf16[16,12,2048]{2,1,0:T(8,128)(2,1)S(1)} async-done(((bf16[16,12,2048]{2,1,0:T(8,128)(2,1)}), bf16[16,12,2048]{2,1,0:T(8,128)(2,1)S(1)}, u32[]{:S(2)}, u32[]{:S(2)}) %all-to-all-start) | async-done | bytes 786464 | tf_op jit(solution)/shard_map/all_to_all | solution.py:36
  46.7 0.2 convert_reduce_fusion
  46.9 0.1 multiply_reduce_fusion
  47.0 0.0 copy-done.6
  47.0 0.1 multiply_convert_fusion
  47.1 1.1 broadcast_in_dim.2
  48.2 3.7 %all-to-all-start.1 = ((bf16[16,12,2048]{2,1,0:T(8,128)(2,1)}), bf16[16,12,2048]{2,1,0:T(8,128)(2,1)S(1)}, u32[]{:S(2)}, u32[]{:S(2)}) async-start(bf16[16,12,2048]{2,1,0:T(8,128)(2,1)} %broadcast_in_dim.2), calls=%async_computation.1 | async-start | bytes 2097152 | tf_op jit(solution)/shard_map/all_to_all | solution.py:42
  51.9 1.7 reduce-window.6
  53.7 0.3 slice_reduce_fusion
  54.0 0.1 fusion.48
  54.1 0.0 copy-start.4
  54.1 0.6 copy-done.4
  54.7 0.1 reduce_sum.84
  54.8 0.1 copy.33
  54.9 1.2 fusion.6
  56.1 9.5 %all-to-all-done.1 = bf16[16,12,2048]{2,1,0:T(8,128)(2,1)S(1)} async-done(((bf16[16,12,2048]{2,1,0:T(8,128)(2,1)}), bf16[16,12,2048]{2,1,0:T(8,128)(2,1)S(1)}, u32[]{:S(2)}, u32[]{:S(2)}) %all-to-all-start.1) | async-done | bytes 786464 | tf_op jit(solution)/shard_map/all_to_all | solution.py:42
  65.7 0.2 reshape.129
  65.8 0.0 copy-done.2
  65.8 0.0 copy-done.3
  65.9 0.4 multiply_reduce_fusion.1
  66.3 7.2 %psum.46 = f32[192]{0:T(256)S(1)} all-reduce(f32[192]{0:T(256)S(1)} %get-tuple-element.47), channel_id=1, replica_groups=mesh['sp'=32,'tp_0'=4,'tp_1'=4] {'tp_0'}, use_global_device_ids=true, to_apply=%region_13.14 | all-reduce | flops 192 | bytes 1536 | tf_op jit(solution)/shard_map/psum | solution.py:24
  73.6 6.6 %psum.47 = f32[192]{0:T(256)S(1)} all-reduce(f32[192]{0:T(256)S(1)} %psum.46), channel_id=1, replica_groups=mesh['sp'=32,'tp_0'=4,'tp_1'=4] {'tp_1'}, use_global_device_ids=true, to_apply=%region_14.15 | all-reduce | flops 192 | bytes 1536 | tf_op jit(solution)/shard_map/psum | solution.py:24
  80.2 1.4 convolution_convert_fusion.1
  81.7 44.6 %all_to_all.30 = bf16[32,32,128]{2,1,0:T(8,128)(2,1)S(1)} all-to-all(bf16[32,32,128]{2,1,0:T(8,128)(2,1)S(1)} %bitcast.176), channel_id=1, replica_groups=mesh['sp'=32,'tp_0'=4,'tp_1'=4] {'sp'}, dimensions={0} | all-to-all | bytes 524288 | tf_op jit(solution)/shard_map/all_to_all | solution.py:124
  126.2 0.8 stack.2
  127.0 0.0 copy-start.9
  127.0 52.8 %all_to_all.31 = bf16[16,32,32,128]{3,2,1,0:T(8,128)(2,1)S(1)} all-to-all(bf16[16,32,32,128]{3,2,1,0:T(8,128)(2,1)S(1)} %stack.2), channel_id=1, replica_groups=mesh['sp'=32,'tp_0'=4,'tp_1'=4] {'tp_0','tp_1'}, dimensions={0} | all-to-all | bytes 8388608 | tf_op jit(solution)/shard_map/all_to_all | solution.py:122
  179.8 1.9 copy-done.1
  181.7 0.0 copy-done.9
  181.7 2.3 fusion.10
  184.1 0.0 copy-done
  184.1 9.1 %convert_bitcast_fusion = bf16[1,32,4,16,8,128]{5,4,3,2,1,0:T(8,128)(2,1)} fusion(bf16[1,256,2048]{2,1,0:T(8,128)(2,1)S(1)} %copy-done, bf16[1,2048,256]{2,1,0:T(8,128)(2,1)} %param.26, f32[32,1,32,256]{3,2,0,1:T(8,128)} %fusion.10, bf16[16,32,32,128]{3,2,1,0:T(8,128)(2,1)} %copy-done.1), kind=kOutput, calls=%fused_computation.6 | convolution fusion | flops 2151940096 | bytes 11534336 | tf_op jit(solution)/shard_map/sjcf,jfd->sjcd/dot_general | solution.py:149
  193.2 3.3 %copy.68 = bf16[1,32,4,16,8,128]{5,4,2,1,0,3:T(8,128)(2,1)S(1)} copy(bf16[1,32,4,16,8,128]{5,4,3,2,1,0:T(8,128)(2,1)} %convert_bitcast_fusion) | data formatting | bytes 8388608 | tf_op jit(solution)/shard_map/reshape | solution.py:30
  196.5 53.1 %all_to_all.32 = bf16[16,32,1,32,128]{4,3,1,2,0:T(8,128)(2,1)} all-to-all(bf16[16,32,1,32,128]{4,3,1,2,0:T(8,128)(2,1)S(1)} %bitcast.173), channel_id=1, replica_groups=mesh['sp'=32,'tp_0'=4,'tp_1'=4] {'tp_0','tp_1'}, dimensions={0} | all-to-all | bytes 8388608 | tf_op jit(solution)/shard_map/all_to_all | solution.py:36
  249.6 3.5 %reduce_sum.86 = bf16[32,32,128]{2,1,0:T(8,128)(2,1)} reduce(bf16[16,32,1,32,128]{4,3,1,2,0:T(8,128)(2,1)} %all_to_all.32, bf16[]{:T(256)} %constant.38.clone.1), dimensions={0,2}, to_apply=%region_15.16 | reduce | flops 1966080 | bytes 4456450 | tf_op jit(solution)/shard_map/reduce_sum | solution.py:37
  253.1 7.2 %all-to-all-start.5 = ((bf16[32,32,128]{2,1,0:T(8,128)(2,1)}), bf16[32,32,128]{2,1,0:T(8,128)(2,1)S(1)}, u32[]{:S(2)}, u32[]{:S(2)}) async-start(bf16[32,32,128]{2,1,0:T(8,128)(2,1)} %reduce_sum.86), calls=%async_computation.5 | async-start | bytes 524288 | tf_op jit(solution)/shard_map/all_to_all | solution.py:153
  260.4 0.1 mul.536
  260.5 0.0 copy-done.8
  260.5 0.1 copy.36
  260.6 0.0 copy-done.5
  260.7 22.0 %all-to-all-done.5 = bf16[32,32,128]{2,1,0:T(8,128)(2,1)S(1)} async-done(((bf16[32,32,128]{2,1,0:T(8,128)(2,1)}), bf16[32,32,128]{2,1,0:T(8,128)(2,1)S(1)}, u32[]{:S(2)}, u32[]{:S(2)}) %all-to-all-start.5) | async-done | bytes 262176 | tf_op jit(solution)/shard_map/all_to_all | solution.py:153
  282.6 1.9 gather_fusion
  284.5 0.3 fusion.45
  284.9 0.6 add_convert_fusion
  (12 shorter events, 0.1 us)
Async XLA Ops:
  0.0 184.1 %copy-start = (bf16[1,256,2048]{2,1,0:T(8,128)(2,1)S(1)}, bf16[1,256,2048]{2,1,0:T(8,128)(2,1)}, u32[]{:S(2)}) copy-start(bf16[1,256,2048]{2,1,0:T(8,128)(2,1)} %param.27) | copy-start | bytes 3145732
  0.0 31.9 %copy-start.7 = (s32[192,4]{0,1:T(4,128)S(1)}, s32[192,4]{0,1:T(4,128)}, u32[]{:S(2)}) copy-start(s32[192,4]{0,1:T(4,128)} %param.23) | copy-start | bytes 9220
  0.0 47.0 %copy-start.6 = (f32[2048]{0:T(1024)S(1)}, f32[2048]{0:T(1024)}, u32[]{:S(2)}) copy-start(f32[2048]{0:T(1024)} %param.20) | copy-start | bytes 24580
  1.0 8.8 %collective-permute-start = (bf16[30,128]{1,0:T(8,128)(2,1)S(1)}, bf16[30,128]{1,0:T(8,128)(2,1)S(1)}, u32[]{:S(2)}, u32[]{:S(2)}) collective-permute-start(bf16[30,128]{1,0:T(8,128)(2,1)S(1)} %slice.258), channel_id=1, source_target_pairs={{0,16},{16,32},{32,48},{48,64},{64,80},{80,96},{96,112},{112,128},... | collective-permute-start | bytes 23048 | tf_op jit(solution)/shard_map/ppermute | solution.py:19
  28.3 18.4 %all-to-all-start = ((bf16[16,12,2048]{2,1,0:T(8,128)(2,1)}), bf16[16,12,2048]{2,1,0:T(8,128)(2,1)S(1)}, u32[]{:S(2)}, u32[]{:S(2)}) async-start(bf16[16,12,2048]{2,1,0:T(8,128)(2,1)} %reshape.128), calls=%async_computation | async-start | bytes 2097152 | tf_op jit(solution)/shard_map/all_to_all | solution.py:36
  31.9 33.9 %copy-start.2 = (bf16[2048,128]{1,0:T(8,128)(2,1)S(1)}, bf16[2048,128]{1,0:T(8,128)(2,1)}, u32[]{:S(2)}) copy-start(bf16[2048,128]{1,0:T(8,128)(2,1)} %param.21) | copy-start | bytes 1572868
  32.0 33.9 %copy-start.3 = (bf16[192,128]{1,0:T(8,128)(2,1)S(1)}, bf16[192,128]{1,0:T(8,128)(2,1)}, u32[]{:S(2)}) copy-start(bf16[192,128]{1,0:T(8,128)(2,1)} %param.14) | copy-start | bytes 147460
  48.2 17.4 %all-to-all-start.1 = ((bf16[16,12,2048]{2,1,0:T(8,128)(2,1)}), bf16[16,12,2048]{2,1,0:T(8,128)(2,1)S(1)}, u32[]{:S(2)}, u32[]{:S(2)}) async-start(bf16[16,12,2048]{2,1,0:T(8,128)(2,1)} %broadcast_in_dim.2), calls=%async_computation.1 | async-start | bytes 2097152 | tf_op jit(solution)/shard_map/all_to_all | solution.py:42
  54.1 0.6 copy-start.4
  127.0 54.7 %copy-start.9 = (bf16[1,2048,256]{2,1,0:T(8,128)(2,1)S(1)}, bf16[1,2048,256]{2,1,0:T(8,128)(2,1)}, u32[]{:S(2)}) copy-start(bf16[1,2048,256]{2,1,0:T(8,128)(2,1)} %param.25) | copy-start | bytes 3145732
  179.8 1.9 copy-start.1
  249.6 10.9 %copy-start.8 = (f32[192,4]{0,1:T(4,128)S(1)}, f32[192,4]{0,1:T(4,128)}, u32[]{:S(2)}) copy-start(f32[192,4]{0,1:T(4,128)} %param.24) | copy-start | bytes 9220
  249.6 11.0 %copy-start.5 = (s32[768]{0:T(1024)S(1)}, s32[768]{0:T(1024)}, u32[]{:S(2)}) copy-start(s32[768]{0:T(1024)} %copy-done.4) | copy-start | bytes 9220
  253.1 29.5 %all-to-all-start.5 = ((bf16[32,32,128]{2,1,0:T(8,128)(2,1)}), bf16[32,32,128]{2,1,0:T(8,128)(2,1)S(1)}, u32[]{:S(2)}, u32[]{:S(2)}) async-start(bf16[32,32,128]{2,1,0:T(8,128)(2,1)} %reduce_sum.86), calls=%async_computation.5 | async-start | bytes 524288 | tf_op jit(solution)/shard_map/all_to_all | solution.py:153
